TPU v7x, 32 devices: a whole 2x2x4 slice. The times are simulated.
32 devices in a mesh: sp: 4 (over z), dp: 8 (over y, x, core).
Axes of the slice: x: 2, y: 2, z: 4, core: 2. Of those that a mesh axis runs over, the one named last changes fastest.
Arguments:
- queries: bfloat16 [8, 512, 1024], P('dp', 'sp'), may hold values from -300 to 300
- keys: bfloat16 [8, 512, 1024], P('dp', 'sp'), may hold values from -7 to 7
- values: bfloat16 [8, 512, 1024], P('dp', 'sp'), may hold values from -6 to 6
- cum_gates: float32 [8, 16, 512], P('dp', 'sp'), may hold values from -67 to 0, as said below
- out_weight: bfloat16 [1024, 2048], P(None, 'dp'), may hold values from -0.1875 to 0.1875
Outputs:
- mixed: bfloat16 [8, 512, 2048], P('dp', 'sp')
Inputs may be any that keep to these rules, and one draw needn't show every extreme that they name: `cum_gates`: never rises along positions.
All inputs are finite; a program needn't handle non-finite values.
Results may differ from a plain program's by a relative error of at most 0.011.
Values may be sent and summed in bfloat16 or wider, within the bound.
A program may use at most 64 MiB of HBM per device.

v0:
```python
import jax
import jax.numpy as jnp
from jax import lax
from jax.sharding import PartitionSpec as P


def attend_heads(query_loc, key_loc, value_loc, cum_loc):
    length = query_loc.shape[0]
    head_count = cum_loc.shape[0]
    head_size = query_loc.shape[1] // head_count
    query_heads = query_loc.reshape(length, head_count, head_size).transpose(1, 0, 2)
    key_heads = key_loc.reshape(length, head_count, head_size).transpose(1, 0, 2)
    value_heads = value_loc.reshape(length, head_count, head_size).transpose(1, 0, 2)
    block_rows = min(512, length)
    block_count = length // block_rows
    query_blocks = query_heads.reshape(head_count, block_count, block_rows, head_size).transpose(
        1, 0, 2, 3
    )
    cum_blocks = cum_loc.reshape(head_count, block_count, block_rows).transpose(1, 0, 2)
    key_pos = jnp.arange(length)
    score_scale = head_size ** (-0.5)

    def one_block(packed):
        query_block, cum_block, block_index = packed
        scores = (
            jnp.einsum("hqd,hkd->hqk", query_block, key_heads, preferred_element_type=jnp.float32)
            * score_scale
        )
        scores = scores + cum_block[:, :, None] - cum_loc[:, None, :]
        query_pos = block_index * block_rows + jnp.arange(block_rows)
        scores = jnp.where(key_pos[None, :] <= query_pos[:, None], scores, -jnp.inf)
        row_max = jnp.max(scores, axis=-1, keepdims=True)
        expon = jnp.exp(scores - row_max)
        weights = (expon / jnp.sum(expon, axis=-1, keepdims=True)).astype(jnp.bfloat16)
        return jnp.einsum(
            "hqk,hkd->hqd", weights, value_heads, preferred_element_type=jnp.float32
        ).astype(jnp.bfloat16)

    results = lax.map(one_block, (query_blocks, cum_blocks, jnp.arange(block_count)))
    return results.transpose(0, 2, 1, 3).reshape(length, head_count * head_size)


def shards(queries, keys, values, cum_gates, out_weight):
    query_loc, key_loc, value_loc = (
        lax.all_to_all(queries[0], "sp", split_axis=1, concat_axis=0, tiled=True),
        lax.all_to_all(keys[0], "sp", split_axis=1, concat_axis=0, tiled=True),
        lax.all_to_all(values[0], "sp", split_axis=1, concat_axis=0, tiled=True),
    )
    head_out = attend_heads(query_loc, key_loc, value_loc, cum_gates[0])
    token_rows = lax.all_to_all(head_out, "sp", split_axis=0, concat_axis=1, tiled=True)
    mixed_rows = jnp.dot(
        token_rows,
        lax.all_gather(out_weight, "dp", axis=1, tiled=True),
        preferred_element_type=jnp.float32,
    )
    return mixed_rows.astype(jnp.bfloat16)[None]


def solution(mesh):
    in_specs = (
        P("dp", "sp", None),
        P("dp", "sp", None),
        P("dp", "sp", None),
        P("dp", "sp", None),
        P(None, "dp"),
    )
    out_specs = P("dp", "sp", None)
    return jax.shard_map(shards, mesh=mesh, in_specs=in_specs, out_specs=out_specs, check_vma=False)
```

profile of v0, /device:TPU:0, one launch (start us, length us, event | category | flops | bytes accessed | tf_op | source)
XLA Modules:
  0.0 70.6 jit_solution(15589185391512869940)
XLA Ops:
  6.5 0.0 all-gather.2.cloned.1.call-start
  6.5 0.7 %all-gather.2.cloned.1.call-update = ((bf16[1024,256]{1,0:T(8,128)(2,1)}), bf16[1024,2048]{1,0:T(8,128)(2,1)}) async-update(((), (), s32[]{:S(2)}) %all-gather.2.cloned.1.call-start, bf16[1024,256]{1,0:T(8,128)(2,1)} %param.9) | async-update | bytes 5242904
  7.3 1.8 %copy.15 = bf16[1,128,1024]{1,2,0:T(8,128)(2,1)} copy(bf16[1,128,1024]{2,1,0:T(8,128)(2,1)} %param.5) | data formatting | bytes 524288 | tf_op args[0]
  9.0 6.3 %all-to-all-start = ((bf16[128,4,256]{0,2,1:T(8,128)(2,1)}), bf16[128,4,256]{0,2,1:T(8,128)(2,1)S(1)}, u32[]{:S(2)}, u32[]{:S(2)}) async-start(bf16[128,4,256]{0,2,1:T(8,128)(2,1)} %bitcast), calls=%async_computation | async-start | bytes 524288 | tf_op jit(solution)/shard_map/all_to_all | solution.py:45
  15.4 1.8 %copy.17 = bf16[1,128,1024]{1,2,0:T(8,128)(2,1)} copy(bf16[1,128,1024]{2,1,0:T(8,128)(2,1)} %param.6) | data formatting | bytes 524288 | tf_op args[1]
  17.2 7.1 %all-to-all-done = bf16[128,4,256]{0,2,1:T(8,128)(2,1)S(1)} async-done(((bf16[128,4,256]{0,2,1:T(8,128)(2,1)}), bf16[128,4,256]{0,2,1:T(8,128)(2,1)S(1)}, u32[]{:S(2)}, u32[]{:S(2)}) %all-to-all-start) | async-done | bytes 262176 | tf_op jit(solution)/shard_map/all_to_all | solution.py:45
  24.3 3.4 %all-to-all-start.1 = ((bf16[128,4,256]{0,2,1:T(8,128)(2,1)}), bf16[128,4,256]{0,2,1:T(8,128)(2,1)S(1)}, u32[]{:S(2)}, u32[]{:S(2)}) async-start(bf16[128,4,256]{0,2,1:T(8,128)(2,1)} %bitcast.3), calls=%async_computation.1 | async-start | bytes 524288 | tf_op jit(solution)/shard_map/all_to_all | solution.py:46
  27.7 1.8 %copy.19 = bf16[1,128,1024]{1,2,0:T(8,128)(2,1)} copy(bf16[1,128,1024]{2,1,0:T(8,128)(2,1)} %param.7) | data formatting | bytes 524288 | tf_op args[2]
  29.5 5.2 %all-to-all-done.1 = bf16[128,4,256]{0,2,1:T(8,128)(2,1)S(1)} async-done(((bf16[128,4,256]{0,2,1:T(8,128)(2,1)}), bf16[128,4,256]{0,2,1:T(8,128)(2,1)S(1)}, u32[]{:S(2)}, u32[]{:S(2)}) %all-to-all-start.1) | async-done | bytes 262176 | tf_op jit(solution)/shard_map/all_to_all | solution.py:46
  34.7 3.4 %all-to-all-start.2 = ((bf16[128,4,256]{0,2,1:T(8,128)(2,1)}), bf16[128,4,256]{0,2,1:T(8,128)(2,1)S(1)}, u32[]{:S(2)}, u32[]{:S(2)}) async-start(bf16[128,4,256]{0,2,1:T(8,128)(2,1)} %bitcast.7), calls=%async_computation.2 | async-start | bytes 524288 | tf_op jit(solution)/shard_map/all_to_all | solution.py:47
  38.1 0.1 iota_compare_fusion
  38.2 0.2 copy.16
  38.4 0.1 reshape.37
  38.5 0.2 copy.18
  38.8 0.1 reshape.38
  38.9 6.0 %all-to-all-done.2 = bf16[128,4,256]{0,2,1:T(8,128)(2,1)S(1)} async-done(((bf16[128,4,256]{0,2,1:T(8,128)(2,1)}), bf16[128,4,256]{0,2,1:T(8,128)(2,1)S(1)}, u32[]{:S(2)}, u32[]{:S(2)}) %all-to-all-start.2) | async-done | bytes 262176 | tf_op jit(solution)/shard_map/all_to_all | solution.py:47
  44.9 0.2 copy.20
  45.1 0.1 reshape.39
  45.2 0.0 copy-done
  45.2 2.2 %fusion.37 = f32[4,512]{1,0:T(4,128)S(1)} fusion(f32[4,512]{1,0:T(4,128)S(1)} %bitcast.61, pred[512,512]{0,1:T(8,128)(4,1)S(1)} %iota_compare_fusion, bf16[512,4,64]{0,2,1:T(8,128)(2,1)S(1)} %reshape.38, bf16[512,4,64]{0,2,1:T(8,128)(2,1)S(1)} %reshape.37), kind=kOutput, calls=%fused_computation.27 | convolution fusion | flops 140509696 | bytes 802816 | tf_op jit(solution)/shard_map/while/body/eval_jaxpr/sub | solution.py:33
  47.4 2.2 %fusion.10 = bf16[1,512,4,64]{1,3,2,0:T(8,128)(2,1)S(1)} fusion(f32[4,512]{1,0:T(4,128)S(1)} %fusion.37, bf16[512,4,64]{0,2,1:T(8,128)(2,1)S(1)} %reshape.39, f32[4,512]{1,0:T(4,128)S(1)} %bitcast.62, pred[512,512]{0,1:T(8,128)(4,1)S(1)} %iota_compare_fusion, bf16[512,4,64]{0,2,1:T(8,128)(2,1)S(1)} %reshape.38, bf16[512,4,64]{0,2,1:T(8,128)(2,1)S(1)} %reshape.37), kind=kOutput, calls=%fused_computation.14 | convolution fusion | flops 275909120 | bytes 1327104 | tf_op jit(solution)/shard_map/while/body/eval_jaxpr/hqk,hkd->hqd/dot_general | solution.py:35
  49.6 0.1 all_to_all.59
  49.7 10.4 %all_to_all.67 = bf16[4,128,256]{1,2,0:T(8,128)(2,1)S(1)} all-to-all(bf16[4,128,256]{1,2,0:T(8,128)(2,1)S(1)} %copy.22), channel_id=1, replica_groups=mesh['sp'=4,'dp'=8] {'sp'}, dimensions={0} | all-to-all | bytes 524288 | tf_op jit(solution)/shard_map/all_to_all | solution.py:50
  60.1 3.7 %fusion.2 = bf16[1,128,2048]{2,1,0:T(8,128)(2,1)} fusion(bf16[128,1024]{0,1:T(8,128)(2,1)S(1)} %bitcast.57, bf16[1024,2048]{1,0:T(8,128)(2,1)} %all-gather.2.cloned.1.call-done), kind=kOutput, calls=%fused_computation.6 | convolution fusion | flops 537133056 | bytes 4980736 | tf_op jit(solution)/shard_map/dot_general | solution.py:51
  (3 shorter events, 0.0 us)
Async XLA Ops:
  6.5 38.7 %copy-start = (f32[1,4,512]{2,1,0:T(4,128)S(1)}, f32[1,4,512]{2,1,0:T(4,128)}, u32[]{:S(2)}) copy-start(f32[1,4,512]{2,1,0:T(4,128)} %param.8) | copy-start | bytes 24580
  6.5 53.5 %all-gather.2.cloned.1.call-start = ((), (), s32[]{:S(2)}) async-start(), calls=%async_computation.4 | async-start | bytes 4718592 | tf_op jit(solution)/shard_map/all_gather | solution.py:53
  9.0 15.3 %all-to-all-start = ((bf16[128,4,256]{0,2,1:T(8,128)(2,1)}), bf16[128,4,256]{0,2,1:T(8,128)(2,1)S(1)}, u32[]{:S(2)}, u32[]{:S(2)}) async-start(bf16[128,4,256]{0,2,1:T(8,128)(2,1)} %bitcast), calls=%async_computation | async-start | bytes 524288 | tf_op jit(solution)/shard_map/all_to_all | solution.py:45
  24.3 10.4 %all-to-all-start.1 = ((bf16[128,4,256]{0,2,1:T(8,128)(2,1)}), bf16[128,4,256]{0,2,1:T(8,128)(2,1)S(1)}, u32[]{:S(2)}, u32[]{:S(2)}) async-start(bf16[128,4,256]{0,2,1:T(8,128)(2,1)} %bitcast.3), calls=%async_computation.1 | async-start | bytes 524288 | tf_op jit(solution)/shard_map/all_to_all | solution.py:46
  34.7 10.2 %all-to-all-start.2 = ((bf16[128,4,256]{0,2,1:T(8,128)(2,1)}), bf16[128,4,256]{0,2,1:T(8,128)(2,1)S(1)}, u32[]{:S(2)}, u32[]{:S(2)}) async-start(bf16[128,4,256]{0,2,1:T(8,128)(2,1)} %bitcast.7), calls=%async_computation.2 | async-start | bytes 524288 | tf_op jit(solution)/shard_map/all_to_all | solution.py:47
Sparse Core Ops, SparseCore 0:
  9.2 40.0 all-gather.1
where the time goes:
time: 71.1 us; the launch traced here: 70.6 us
  waiting for transfers between devices  19.1 us (27%)
  between operations  13.5 us (19%)
  starting transfers between devices  13.2 us (19%)
  blocking collectives  10.4 us (15%)
  matrix products  8.1 us (11%)
  local copies, waits for them, and re-layouts  6.39 us (9%)
    all_to_all x1, blocking collectives, shards(): lax.all_to_all(head_out, 'sp', split_axis=0, concat_axis=1, tiled=True)  10.4 us
    all_to_all x1, waiting for transfers between devices, shards(): lax.all_to_all(queries[0], 'sp', split_axis=1, concat_axis=0, tiled=True)  7.12 us
    all_to_all x1, starting transfers between devices, shards(): lax.all_to_all(queries[0], 'sp', split_axis=1, concat_axis=0, tiled=True)  6.35 us
    all_to_all x1, waiting for transfers between devices, shards(): lax.all_to_all(values[0], 'sp', split_axis=1, concat_axis=0, tiled=True)  6.01 us
    unnamed x5, local copies, waits for them, and re-layouts  5.36 us
    all_to_all x1, waiting for transfers between devices, shards(): lax.all_to_all(keys[0], 'sp', split_axis=1, concat_axis=0, tiled=True)  5.21 us
    dot_general x1, matrix products, shards(): jnp.dot(token_rows, lax.all_gather(out_weight, 'dp', axis=1, tiled=True),...  3.72 us
    all_to_all x1, starting transfers between devices, shards(): lax.all_to_all(keys[0], 'sp', split_axis=1, concat_axis=0, tiled=True)  3.41 us
  transfers between devices with their start and end apart: 4, of which 3 were waited for; matrix products, arithmetic and copies ran while one was open for 15% of the time, Pallas kernels for 0%

commit v1 on v0

--- a/solution.py
+++ b/solution.py
@@ -44,7 +44,12 @@
     query_loc, key_loc, value_loc = (
         lax.all_to_all(queries[0], "sp", split_axis=1, concat_axis=0, tiled=True),
         lax.all_to_all(keys[0], "sp", split_axis=1, concat_axis=0, tiled=True),
-        lax.all_to_all(values[0], "sp", split_axis=1, concat_axis=0, tiled=True),
+        jnp.concatenate(
+            lax.all_to_all(
+                jnp.stack(jnp.split(values[0], lax.axis_size("sp"), axis=1)), "sp", 0, 0
+            ),
+            axis=0,
+        ),
     )
     head_out = attend_heads(query_loc, key_loc, value_loc, cum_gates[0])
     token_rows = lax.all_to_all(head_out, "sp", split_axis=0, concat_axis=1, tiled=True)

time: 71.1 us -> 71.1 us (level)
  local copies, waits for them, and re-layouts: 6.39 us -> 5.54 us
  other arithmetic: 0.08 us -> 0.82 us
    all_to_all x1, starting transfers between devices: 3.4 us -> 6.35 us  [shards(): lax.all_to_all(jnp.stack(jnp.split(values[0], lax.axis_size('sp'), axis=1...]
    all_to_all x1, starting transfers between devices: 6.35 us -> 3.4 us  [shards(): lax.all_to_all(queries[0], 'sp', split_axis=1, concat_axis=0, tiled=True)]
    all_to_all x1, waiting for transfers between devices: 7.12 us -> 5.21 us  [shards(): lax.all_to_all(queries[0], 'sp', split_axis=1, concat_axis=0, tiled=True)]
    unnamed x5 -> x4, local copies, waits for them, and re-layouts: 5.36 us -> 3.57 us
    all_to_all x1, waiting for transfers between devices: 6.01 us -> 7.13 us  [shards(): lax.all_to_all(jnp.stack(jnp.split(values[0], lax.axis_size('sp'), axis=1...]
    another operation x0 -> x2, local copies, waits for them, and re-layouts: none -> 1.06 us  [the longest x1 0.96 us: shards(): jnp.stack(jnp.split(values[0], lax.axis_size('sp'), axis=1))]
    all_to_all x1, waiting for transfers between devices: 5.21 us -> 6.03 us  [shards(): lax.all_to_all(keys[0], 'sp', split_axis=1, concat_axis=0, tiled=True)]
    another operation x0 -> x1, other arithmetic: none -> 0.74 us  [shards(): jnp.stack(jnp.split(values[0], lax.axis_size('sp'), axis=1))]
where the time goes in v1:
time: 71.1 us; the launch traced here: 70.5 us
  waiting for transfers between devices  19.1 us (27%)
  between operations  13.5 us (19%)
  starting transfers between devices  13.2 us (19%)
  blocking collectives  10.4 us (15%)
  matrix products  8.1 us (11%)
  local copies, waits for them, and re-layouts  5.54 us (8%)
  other arithmetic  0.82 us (1%)
    all_to_all x1, blocking collectives, shards(): lax.all_to_all(head_out, 'sp', split_axis=0, concat_axis=1, tiled=True)  10.4 us
    all_to_all x1, waiting for transfers between devices, shards(): lax.all_to_all(jnp.stack(jnp.split(values[0], lax.axis_size('sp'), axis=1...  7.13 us
    all_to_all x1, starting transfers between devices, shards(): lax.all_to_all(jnp.stack(jnp.split(values[0], lax.axis_size('sp'), axis=1...  6.35 us
    all_to_all x1, waiting for transfers between devices, shards(): lax.all_to_all(keys[0], 'sp', split_axis=1, concat_axis=0, tiled=True)  6.03 us
    all_to_all x1, waiting for transfers between devices, shards(): lax.all_to_all(queries[0], 'sp', split_axis=1, concat_axis=0, tiled=True)  5.21 us
    dot_general x1, matrix products, shards(): jnp.dot(token_rows, lax.all_gather(out_weight, 'dp', axis=1, tiled=True),...  3.73 us
    unnamed x4, local copies, waits for them, and re-layouts  3.57 us
    all_to_all x1, starting transfers between devices, shards(): lax.all_to_all(keys[0], 'sp', split_axis=1, concat_axis=0, tiled=True)  3.41 us
  transfers between devices with their start and end apart: 4, of which 3 were waited for; matrix products, arithmetic and copies ran while one was open for 15% of the time, Pallas kernels for 0%

profile of v1, /device:TPU:0, one launch (start us, length us, event | category | flops | bytes accessed | tf_op | source)
XLA Modules:
  0.0 70.5 jit_solution(1021142222102623833)
XLA Ops:
  6.5 0.0 all-gather.2.cloned.1.call-start
  6.5 0.7 %all-gather.2.cloned.1.call-update = ((bf16[1024,256]{1,0:T(8,128)(2,1)}), bf16[1024,2048]{1,0:T(8,128)(2,1)}) async-update(((), (), s32[]{:S(2)}) %all-gather.2.cloned.1.call-start, bf16[1024,256]{1,0:T(8,128)(2,1)} %param.9) | async-update | bytes 5242904
  7.3 1.0 %slice_bitcast_fusion.3 = (bf16[1,128,256]{2,1,0:T(8,128)(2,1)S(1)}, bf16[1,128,256]{2,1,0:T(8,128)(2,1)S(1)}, bf16[1,128,256]{2,1,0:T(8,128)(2,1)S(1)}, bf16[1,128,256]{2,1,0:T(8,128)(2,1)S(1)}) fusion(bf16[128,1024]{1,0:T(8,128)(2,1)} %bitcast.67), kind=kLoop, calls=%fused_computation.27 | loop fusion | bytes 524288 | tf_op jit(solution)/shard_map/stack | solution.py:49
  8.2 0.7 %pad_maximum_fusion = bf16[4,128,256]{2,1,0:T(8,128)(2,1)} fusion(bf16[1,128,256]{2,1,0:T(8,128)(2,1)S(1)} %get-tuple-element.18, bf16[1,128,256]{2,1,0:T(8,128)(2,1)S(1)} %get-tuple-element.19, bf16[1,128,256]{2,1,0:T(8,128)(2,1)S(1)} %get-tuple-element.20, bf16[1,128,256]{2,1,0:T(8,128)(2,1)S(1)} %get-tuple-element.17), kind=kLoop, calls=%fused_computation.17 | loop fusion | flops 393216 | bytes 524288 | tf_op jit(solution)/shard_map/stack | solution.py:49
  9.0 6.3 %all-to-all-start.2 = ((bf16[4,128,256]{2,1,0:T(8,128)(2,1)}), bf16[4,128,256]{2,1,0:T(8,128)(2,1)S(1)}, u32[]{:S(2)}, u32[]{:S(2)}) async-start(bf16[4,128,256]{2,1,0:T(8,128)(2,1)} %pad_maximum_fusion), calls=%async_computation.2 | async-start | bytes 524288 | tf_op jit(solution)/shard_map/all_to_all | solution.py:48
  15.3 1.8 %copy.15 = bf16[1,128,1024]{1,2,0:T(8,128)(2,1)} copy(bf16[1,128,1024]{2,1,0:T(8,128)(2,1)} %param.5) | data formatting | bytes 524288 | tf_op args[0]
  17.1 7.1 %all-to-all-done.2 = bf16[4,128,256]{2,1,0:T(8,128)(2,1)S(1)} async-done(((bf16[4,128,256]{2,1,0:T(8,128)(2,1)}), bf16[4,128,256]{2,1,0:T(8,128)(2,1)S(1)}, u32[]{:S(2)}, u32[]{:S(2)}) %all-to-all-start.2) | async-done | bytes 262176 | tf_op jit(solution)/shard_map/all_to_all | solution.py:48
  24.2 3.4 %all-to-all-start = ((bf16[128,4,256]{0,2,1:T(8,128)(2,1)}), bf16[128,4,256]{0,2,1:T(8,128)(2,1)S(1)}, u32[]{:S(2)}, u32[]{:S(2)}) async-start(bf16[128,4,256]{0,2,1:T(8,128)(2,1)} %bitcast), calls=%async_computation | async-start | bytes 524288 | tf_op jit(solution)/shard_map/all_to_all | solution.py:45
  27.6 1.8 %copy.17 = bf16[1,128,1024]{1,2,0:T(8,128)(2,1)} copy(bf16[1,128,1024]{2,1,0:T(8,128)(2,1)} %param.6) | data formatting | bytes 524288 | tf_op args[1]
  29.4 5.2 %all-to-all-done = bf16[128,4,256]{0,2,1:T(8,128)(2,1)S(1)} async-done(((bf16[128,4,256]{0,2,1:T(8,128)(2,1)}), bf16[128,4,256]{0,2,1:T(8,128)(2,1)S(1)}, u32[]{:S(2)}, u32[]{:S(2)}) %all-to-all-start) | async-done | bytes 262176 | tf_op jit(solution)/shard_map/all_to_all | solution.py:45
  34.6 3.4 %all-to-all-start.1 = ((bf16[128,4,256]{0,2,1:T(8,128)(2,1)}), bf16[128,4,256]{0,2,1:T(8,128)(2,1)S(1)}, u32[]{:S(2)}, u32[]{:S(2)}) async-start(bf16[128,4,256]{0,2,1:T(8,128)(2,1)} %bitcast.3), calls=%async_computation.1 | async-start | bytes 524288 | tf_op jit(solution)/shard_map/all_to_all | solution.py:46
  38.0 0.1 iota_compare_fusion
  38.1 0.2 copy.19
  38.3 0.1 reshape_reshape.3
  38.4 0.2 copy.16
  38.6 0.1 reshape.29
  38.8 6.0 %all-to-all-done.1 = bf16[128,4,256]{0,2,1:T(8,128)(2,1)S(1)} async-done(((bf16[128,4,256]{0,2,1:T(8,128)(2,1)}), bf16[128,4,256]{0,2,1:T(8,128)(2,1)S(1)}, u32[]{:S(2)}, u32[]{:S(2)}) %all-to-all-start.1) | async-done | bytes 262176 | tf_op jit(solution)/shard_map/all_to_all | solution.py:46
  44.8 0.2 copy.18
  45.0 0.1 reshape.30
  45.1 2.2 %fusion.37 = f32[4,512]{1,0:T(4,128)S(1)} fusion(f32[4,512]{1,0:T(4,128)S(1)} %bitcast.68, pred[512,512]{0,1:T(8,128)(4,1)S(1)} %iota_compare_fusion, bf16[512,4,64]{0,2,1:T(8,128)(2,1)S(1)} %reshape.30, bf16[512,4,64]{0,2,1:T(8,128)(2,1)S(1)} %reshape.29), kind=kOutput, calls=%fused_computation.32 | convolution fusion | flops 140509696 | bytes 802816 | tf_op jit(solution)/shard_map/while/body/eval_jaxpr/sub | solution.py:33
  47.3 2.2 %fusion.10 = bf16[1,512,4,64]{1,3,2,0:T(8,128)(2,1)S(1)} fusion(f32[4,512]{1,0:T(4,128)S(1)} %fusion.37, bf16[512,4,64]{0,2,1:T(8,128)(2,1)S(1)} %reshape_reshape.3, f32[4,512]{1,0:T(4,128)S(1)} %bitcast.69, pred[512,512]{0,1:T(8,128)(4,1)S(1)} %iota_compare_fusion, bf16[512,4,64]{0,2,1:T(8,128)(2,1)S(1)} %reshape.30, bf16[512,4,64]{0,2,1:T(8,128)(2,1)S(1)} %reshape.29), kind=kOutput, calls=%fused_computation.14 | convolution fusion | flops 275909120 | bytes 1327104 | tf_op jit(solution)/shard_map/while/body/eval_jaxpr/hqk,hkd->hqd/dot_general | solution.py:35
  49.5 0.1 all_to_all.48
  49.6 10.4 %all_to_all.56 = bf16[4,128,256]{1,2,0:T(8,128)(2,1)S(1)} all-to-all(bf16[4,128,256]{1,2,0:T(8,128)(2,1)S(1)} %copy.21), channel_id=1, replica_groups=mesh['sp'=4,'dp'=8] {'sp'}, dimensions={0} | all-to-all | bytes 524288 | tf_op jit(solution)/shard_map/all_to_all | solution.py:55
  60.0 3.7 %fusion.2 = bf16[1,128,2048]{2,1,0:T(8,128)(2,1)} fusion(bf16[128,1024]{0,1:T(8,128)(2,1)S(1)} %bitcast.64, bf16[1024,2048]{1,0:T(8,128)(2,1)} %all-gather.2.cloned.1.call-done), kind=kOutput, calls=%fused_computation.6 | convolution fusion | flops 537133056 | bytes 4980736 | tf_op jit(solution)/shard_map/dot_general | solution.py:56
  (4 shorter events, 0.0 us)
Async XLA Ops:
  6.5 38.6 %copy-start = (f32[1,4,512]{2,1,0:T(4,128)S(1)}, f32[1,4,512]{2,1,0:T(4,128)}, u32[]{:S(2)}) copy-start(f32[1,4,512]{2,1,0:T(4,128)} %param.8) | copy-start | bytes 24580
  6.5 53.4 %all-gather.2.cloned.1.call-start = ((), (), s32[]{:S(2)}) async-start(), calls=%async_computation.4 | async-start | bytes 4718592 | tf_op jit(solution)/shard_map/all_gather | solution.py:58
  9.0 15.3 %all-to-all-start.2 = ((bf16[4,128,256]{2,1,0:T(8,128)(2,1)}), bf16[4,128,256]{2,1,0:T(8,128)(2,1)S(1)}, u32[]{:S(2)}, u32[]{:S(2)}) async-start(bf16[4,128,256]{2,1,0:T(8,128)(2,1)} %pad_maximum_fusion), calls=%async_computation.2 | async-start | bytes 524288 | tf_op jit(solution)/shard_map/all_to_all | solution.py:48
  24.2 10.4 %all-to-all-start = ((bf16[128,4,256]{0,2,1:T(8,128)(2,1)}), bf16[128,4,256]{0,2,1:T(8,128)(2,1)S(1)}, u32[]{:S(2)}, u32[]{:S(2)}) async-start(bf16[128,4,256]{0,2,1:T(8,128)(2,1)} %bitcast), calls=%async_computation | async-start | bytes 524288 | tf_op jit(solution)/shard_map/all_to_all | solution.py:45
  34.6 10.2 %all-to-all-start.1 = ((bf16[128,4,256]{0,2,1:T(8,128)(2,1)}), bf16[128,4,256]{0,2,1:T(8,128)(2,1)S(1)}, u32[]{:S(2)}, u32[]{:S(2)}) async-start(bf16[128,4,256]{0,2,1:T(8,128)(2,1)} %bitcast.3), calls=%async_computation.1 | async-start | bytes 524288 | tf_op jit(solution)/shard_map/all_to_all | solution.py:46
Sparse Core Ops, SparseCore 0:
  9.2 40.0 all-gather.1
